TPU v7x, 32 devices: a whole 2x2x4 slice. The times are simulated.
32 devices in a mesh: fs: 4 (over z), rep: 4 (over y, x), tp: 2 (over core).
Axes of the slice: x: 2, y: 2, z: 4, core: 2. Of those that a mesh axis runs over, the one named last changes fastest.
Arguments:
- first_mix: bfloat16 [12288, 2048], P(('fs', 'rep'), 'tp'), may hold values from -6 to 6
- second_mix: bfloat16 [12288, 2048], P(('fs', 'rep'), 'tp'), may hold values from -6 to 6
- lambda_head: float32 [8], P('tp'), may hold values from 0.3 to 0.8
- head_gain: float32 [256], replicated, may hold values from 0.1 to 1.9
- out_cotangent: bfloat16 [12288, 2048], P(('fs', 'rep')), may hold values from -0.053955078 to 0.053955078
- basis: bfloat16 [2048, 256], P('tp'), may hold values from -0.125 to 0.125
- weight: float32 [2048, 2048], P('tp', 'fs'), may hold values from -3 to 3
- first_moment: float32 [2048, 256], P('fs', 'tp'), may hold values from -4.5 to 4.5
- second_moment: float32 [2048, 256], P('fs', 'tp'), may hold values from 0.05 to 0.5
Outputs:
- weight_new: float32 [2048, 2048], P('tp', 'fs')
- weight_copy: bfloat16 [2048, 2048], P('tp')
- step_out: float32 [2048, 2048], P('tp', 'fs')
- first_new: float32 [2048, 256], P('fs', 'tp')
- second_new: float32 [2048, 256], P('fs', 'tp')
All inputs are finite; a program needn't handle non-finite values.
Results may differ from a plain program's by a relative error of at most 0.0075.
Values may be sent and summed in bfloat16 or wider, within the bound.
A program may use at most 64 MiB of HBM per device.

v0:
```python
import jax
import jax.numpy as jnp
from jax import lax
from jax.sharding import PartitionSpec as P

out_scale = 0.8
beta_first = 0.9
beta_second = 0.95


def head_output(first_piece, second_piece, lambdas, head_gain):
    token_count = first_piece.shape[0]
    head_width = head_gain.shape[0]
    head_count = lambdas.shape[0] // head_width
    mixture = first_piece.astype(jnp.float32) - lambdas[None, :] * second_piece.astype(jnp.float32)
    grouped = mixture.reshape(token_count, head_count, head_width)
    inverse = lax.rsqrt(jnp.mean(grouped * grouped, axis=-1, keepdims=True) + 1e-06)
    normed = grouped * inverse * head_gain[None, None, :] * out_scale
    return normed.reshape(token_count, head_count * head_width).astype(jnp.bfloat16)


def split_product(narrow, wide, numbers):
    upper = wide.astype(jnp.bfloat16)
    lower = (wide - upper.astype(jnp.float32)).astype(jnp.bfloat16)
    return lax.dot_general(
        narrow, upper, numbers, preferred_element_type=jnp.float32
    ) + lax.dot_general(narrow, lower, numbers, preferred_element_type=jnp.float32)


def body(
    first_mix,
    second_mix,
    lambda_head,
    head_gain,
    out_cotangent,
    basis,
    weight,
    first_moment,
    second_moment,
):
    lambdas = jnp.repeat(lambda_head, head_gain.shape[0])
    head_out = head_output(first_mix, second_mix, lambdas, head_gain)
    reduced = jnp.dot(head_out, basis, preferred_element_type=jnp.float32)
    proj_rows = lax.psum_scatter(
        split_product(out_cotangent, reduced, (((0,), (0,)), ((), ()))),
        "fs",
        scatter_dimension=0,
        tiled=True,
    )
    proj_rows = lax.psum_scatter(proj_rows, "tp", scatter_dimension=1, tiled=True)
    projected = lax.psum(proj_rows, "rep")
    first_new = beta_first * first_moment + (1.0 - beta_first) * projected
    second_new = beta_second * second_moment + (1.0 - beta_second) * projected * projected
    direction = first_new / (jnp.sqrt(second_new) + 1e-08)
    energy = lax.psum(jnp.sum(direction * direction), ("fs", "tp"))
    entries = direction.shape[0] * direction.shape[1] * lax.axis_size("fs") * lax.axis_size("tp")
    spread = jnp.sqrt(energy / entries)
    full_direction = lax.all_gather(direction, "tp", axis=1, tiled=True)
    step_out = split_product(basis, full_direction, (((1,), (1,)), ((), ()))) * (
        -1.0 / (spread + 1e-06)
    )
    weight_new = weight + step_out
    weight_copy = lax.all_gather(weight_new.astype(jnp.bfloat16), "fs", axis=1, tiled=True)
    return (weight_new, weight_copy, step_out, first_new, second_new)


def solution(mesh):
    return jax.shard_map(
        body,
        mesh=mesh,
        in_specs=(
            P(("fs", "rep"), "tp"),
            P(("fs", "rep"), "tp"),
            P("tp"),
            P(),
            P(("fs", "rep"), None),
            P("tp", None),
            P("tp", "fs"),
            P("fs", "tp"),
            P("fs", "tp"),
        ),
        out_specs=(P("tp", "fs"), P("tp", None), P("tp", "fs"), P("fs", "tp"), P("fs", "tp")),
        check_vma=False,
    )
```

profile of v0, /device:TPU:0, one launch (start us, length us, event | category | flops | bytes accessed | tf_op | source)
XLA Modules:
  0.0 254.0 jit_solution(11689265764747644795)
XLA Ops:
  7.2 0.9 broadcast_bitcast_fusion.1
  8.1 0.7 broadcast_bitcast_fusion
  8.8 4.2 %fusion = f32[768,1024]{1,0:T(8,128)} fusion(bf16[768,1024]{1,0:T(8,128)(2,1)} %param.10, bf16[768,1024]{1,0:T(8,128)(2,1)} %param.9, f32[1024]{0:T(1024)S(1)} %bitcast.19), kind=kLoop, calls=%fused_computation.2 | loop fusion | flops 3932160 | bytes 6295552 | tf_op jit(solution)/shard_map/mul | solution.py:17
  13.0 5.2 %mul.92 = f32[768,4,256]{2,1,0:T(4,128)} reshape(f32[768,1024]{1,0:T(8,128)} %fusion) | data formatting | bytes 6291456 | tf_op jit(solution)/shard_map/mul | solution.py:17
  18.2 2.8 %reduce_sum.18 = f32[768,4]{1,0:T(8,128)S(1)} reduce(f32[768,4,256]{2,1,0:T(4,128)} %mul.92, f32[]{:T(128)} %constant.2.clone.1), dimensions={2}, to_apply=%region_0.0 | reduce | flops 783360 | bytes 3158020 | tf_op jit(solution)/shard_map/reduce_sum | solution.py:17
  21.0 0.1 add_rsqrt_fusion
  21.1 1.0 mul.93
  22.1 0.8 copy.42
  22.8 0.6 copy-done.1
  23.5 0.5 copy-done.2
  23.9 0.1 copy-done.3
  24.0 0.9 fusion.2
  25.0 1.0 fusion.5
  26.0 2.4 fusion.1
  28.5 46.5 %reduce-scatter.3.cloned.1.call-done = f32[512,256]{0,1:T(8,128)} async-done(((f32[2048,256]{0,1:T(8,128)}), f32[512,256]{0,1:T(8,128)}) %reduce-scatter.3.cloned.1.call-update) | async-done | bytes 524304 | tf_op jit(solution)/shard_map/reduce_scatter | solution.py:44
  75.0 9.3 %reduce-scatter.5.cloned.1.call-done = f32[512,128]{0,1:T(8,128)} async-done(((f32[512,256]{0,1:T(8,128)}), f32[512,128]{0,1:T(8,128)}) %reduce-scatter.5.cloned.1.call-update) | async-done | bytes 262160 | tf_op jit(solution)/shard_map/reduce_scatter | solution.py:50
  84.4 0.8 copy.31
  85.2 1.8 copy.34
  87.0 2.9 %copy.35 = f32[1024,512]{0,1:T(8,128)} copy(f32[1024,512]{1,0:T(8,128)} %param.15) | data formatting | bytes 4194304 | tf_op args[6]
  89.9 41.6 %all-reduce.2.cloned.1.call-done = f32[512,128]{0,1:T(8,128)} async-done(((f32[512,128]{0,1:T(8,128)}), f32[512,128]{0,1:T(8,128)}) %all-reduce.2.cloned.1.call-update) | async-done | bytes 262160 | tf_op jit(solution)/shard_map/psum | solution.py:51
  131.5 2.6 %multiply_reduce_fusion = (f32[]{:T(128)}, f32[512,128]{0,1:T(8,128)S(1)}, f32[512,128]{0,1:T(8,128)}, f32[512,128]{0,1:T(8,128)}) fusion(f32[512,128]{0,1:T(8,128)} %all-reduce.2.cloned.1.call-done, f32[512,128]{0,1:T(8,128)} %copy.34, f32[512,128]{0,1:T(8,128)} %copy.31), kind=kLoop, calls=%fused_computation.12 | loop fusion | flops 720895 | bytes 1572868 | tf_op jit(solution)/shard_map/reduce_sum | solution.py:55
  134.1 16.5 %psum.15 = f32[]{:T(128)} all-reduce(f32[]{:T(128)} %get-tuple-element.22), channel_id=1, replica_groups=mesh['fs'=4,'rep'=4,'tp'=2] {'fs','tp'}, use_global_device_ids=true, to_apply=%region_5.0 | all-reduce | flops 1 | bytes 8 | tf_op jit(solution)/shard_map/psum | solution.py:55
  151.3 2.2 all_gather.6
  153.5 0.8 copy-done.4
  154.3 2.8 %fusion.8 = f32[512,1024]{1,0:T(8,128)} fusion(bf16[1024,256]{1,0:T(8,128)(2,1)} %param.14, f32[512,256]{0,1:T(8,128)S(1)} %all_gather.6), kind=kOutput, calls=%fused_computation.19 | convolution fusion | flops 268566528 | bytes 3145728 | tf_op jit(solution)/shard_map/dot_general | solution.py:25
  157.2 5.7 %fusion.11 = (bf16[1024,512]{0,1:T(8,128)(2,1)}, f32[1024,512]{0,1:T(8,128)}, f32[1024,512]{0,1:T(8,128)}) fusion(f32[1024,512]{0,1:T(8,128)} %copy.35, f32[]{:T(128)S(6)} %div.19, f32[512,1024]{1,0:T(8,128)} %fusion.8, bf16[1024,256]{1,0:T(8,128)(2,1)} %param.14, f32[512,256]{0,1:T(8,128)} %copy-done.4), kind=kOutput, calls=%fused_computation.24 | convolution fusion | flops 271056896 | bytes 10485764 | tf_op jit(solution)/shard_map/dot_general | solution.py:27
  162.9 1.8 copy.40
  164.7 0.8 copy.39
  165.5 3.0 %copy.36 = f32[1024,512]{1,0:T(8,128)} copy(f32[1024,512]{0,1:T(8,128)} %get-tuple-element.21) | data formatting | bytes 4194304
  168.5 3.0 %copy.38 = f32[1024,512]{1,0:T(8,128)} copy(f32[1024,512]{0,1:T(8,128)} %get-tuple-element.26) | data formatting | bytes 4194304
  171.5 69.5 %all-gather.2.cloned.1.call-done = bf16[1024,2048]{0,1:T(8,128)(2,1)} async-done(((bf16[1024,512]{0,1:T(8,128)(2,1)}), bf16[1024,2048]{0,1:T(8,128)(2,1)}) %all-gather.2.cloned.1.call-update) | async-done | bytes 4194320 | tf_op jit(solution)/shard_map/all_gather | solution.py:63
  241.0 6.4 %copy.37 = bf16[1024,2048]{1,0:T(8,128)(2,1)} copy(bf16[1024,2048]{0,1:T(8,128)(2,1)} %all-gather.2.cloned.1.call-done) | data formatting | bytes 8388608
  (20 shorter events, 0.3 us)
Async XLA Ops:
  7.2 17.8 %copy-start = (bf16[768,2048]{1,0:T(8,128)(2,1)S(1)}, bf16[768,2048]{1,0:T(8,128)(2,1)}, u32[]{:S(2)}) copy-start(bf16[768,2048]{1,0:T(8,128)(2,1)} %param.13) | copy-start | bytes 9437188
  7.2 67.7 %reduce-scatter.3.cloned.1.call-start = ((), (), s32[]{:S(2)}) async-start(), calls=%async_computation.2 | async-start | bytes 2621440 | tf_op jit(solution)/shard_map/reduce_scatter | solution.py:44
  22.0 1.4 copy-start.1
  22.1 1.9 copy-start.2
  22.1 2.0 copy-start.3
  26.0 58.4 %copy-start.6 = (f32[512,128]{1,0:T(8,128)S(1)}, f32[512,128]{1,0:T(8,128)}, u32[]{:S(2)}) copy-start(f32[512,128]{1,0:T(8,128)} %param.16) | copy-start | bytes 786436
  28.4 55.9 %reduce-scatter.5.cloned.1.call-start = ((), (), s32[]{:S(2)}) async-start(), calls=%async_computation.3 | async-start | bytes 786432 | tf_op jit(solution)/shard_map/reduce_scatter | solution.py:50
  74.9 56.5 %all-reduce.2.cloned.1.call-start = ((), (), s32[]{:S(2)}) async-start(), calls=%async_computation.4 | async-start | bytes 524288 | tf_op jit(solution)/shard_map/psum | solution.py:51
  84.4 156.6 %all-gather.2.cloned.1.call-start = ((), (), s32[]{:S(2)}) async-start(), calls=%async_computation.5 | async-start | bytes 5242880 | tf_op jit(solution)/shard_map/all_gather | solution.py:63
  153.5 0.8 copy-start.4
  157.2 7.5 %copy-start.5 = (f32[512,128]{0,1:T(8,128)S(1)}, f32[512,128]{0,1:T(8,128)}, u32[]{:S(2)}) copy-start(f32[512,128]{0,1:T(8,128)} %get-tuple-element.25) | copy-start | bytes 786436
Sparse Core Ops, SparseCore 0:
  28.5 46.3 reduce-scatter.2
  77.2 7.1 reduce-scatter.4
  87.3 44.1 all-reduce.1
  163.0 77.9 all-gather.1
where the time goes:
time: 255 us; the launch traced here: 254 us
  waiting for transfers between devices  167 us (65%)
  local copies, waits for them, and re-layouts  31 us (12%)
  blocking collectives  18.7 us (7%)
  between operations  14.6 us (6%)
  matrix products  12.8 us (5%)
  other arithmetic  9.72 us (4%)
    all_gather x1, waiting for transfers between devices, body(): lax.all_gather(weight_new.astype(jnp.bfloat16), 'fs', axis=1, tiled=True)  69.5 us
    reduce_scatter x1, waiting for transfers between devices, body(): lax.psum_scatter(split_product(out_cotangent, reduced, (((0,), (0,)), (()...  46.5 us
    psum x1, waiting for transfers between devices, body(): projected = lax.psum(proj_rows, 'rep')  41.6 us
    unnamed x27, local copies, waits for them, and re-layouts  24.9 us
    psum x1, blocking collectives, body(): energy = lax.psum(jnp.sum(direction * direction), ('fs', 'tp'))  16.5 us
    reduce_scatter x1, waiting for transfers between devices, body(): lax.psum_scatter(proj_rows, 'tp', scatter_dimension=1, tiled=True)  9.34 us
    dot_general x2, matrix products, split_product(): lax.dot_general(narrow, lower, numbers, preferred_element_type=jnp.float32)  8.03 us
    mul x1, local copies, waits for them, and re-layouts, head_output(): grouped * grouped  5.15 us
  transfers between devices with their start and end apart: 4, of which 4 were waited for; matrix products, arithmetic and copies ran while one was open for 6% of the time, Pallas kernels for 0%

commit v1 on v0

--- a/solution.py
+++ b/solution.py
@@ -6,6 +6,12 @@
 out_scale = 0.8
 beta_first = 0.9
 beta_second = 0.95
+
+
+def summed_here(block, name):
+    parts = lax.all_gather(block, name, axis=0, tiled=False)
+    summed = parts.sum(axis=0)
+    return summed
 
 
 def head_output(first_piece, second_piece, lambdas, head_gain):
@@ -48,7 +54,7 @@
         tiled=True,
     )
     proj_rows = lax.psum_scatter(proj_rows, "tp", scatter_dimension=1, tiled=True)
-    projected = lax.psum(proj_rows, "rep")
+    projected = summed_here(proj_rows, "rep")
     first_new = beta_first * first_moment + (1.0 - beta_first) * projected
     second_new = beta_second * second_moment + (1.0 - beta_second) * projected * projected
     direction = first_new / (jnp.sqrt(second_new) + 1e-08)

time: 255 us -> 243 us (0.953)
  waiting for transfers between devices: 167 us -> 149 us
  local copies, waits for them, and re-layouts: 31 us -> 33.9 us
  other arithmetic: 9.72 us -> 12.3 us
    psum x1 -> x0, waiting for transfers between devices: 41.6 us -> none  [body(): projected = lax.psum(proj_rows, 'rep')]
    all_gather x0 -> x1, waiting for transfers between devices: none -> 23.9 us  [summed_here(): parts = lax.all_gather(block, name, axis=0, tiled=False)]
    all_gather x0 -> x1, local copies, waits for them, and re-layouts: none -> 2.9 us  [summed_here(): parts = lax.all_gather(block, name, axis=0, tiled=False)]
where the time goes in v1:
time: 243 us; the launch traced here: 242 us
  waiting for transfers between devices  149 us (61%)
  local copies, waits for them, and re-layouts  33.9 us (14%)
  blocking collectives  19 us (8%)
  between operations  14.6 us (6%)
  matrix products  12.8 us (5%)
  other arithmetic  12.3 us (5%)
    all_gather x1, waiting for transfers between devices, body(): lax.all_gather(weight_new.astype(jnp.bfloat16), 'fs', axis=1, tiled=True)  69.5 us
    reduce_scatter x1, waiting for transfers between devices, body(): lax.psum_scatter(split_product(out_cotangent, reduced, (((0,), (0,)), (()...  46.5 us
    unnamed x27, local copies, waits for them, and re-layouts  24.9 us
    all_gather x1, waiting for transfers between devices, summed_here(): parts = lax.all_gather(block, name, axis=0, tiled=False)  23.9 us
    psum x1, blocking collectives, body(): energy = lax.psum(jnp.sum(direction * direction), ('fs', 'tp'))  16.8 us
    reduce_scatter x1, waiting for transfers between devices, body(): lax.psum_scatter(proj_rows, 'tp', scatter_dimension=1, tiled=True)  9.34 us
    dot_general x2, matrix products, split_product(): lax.dot_general(narrow, lower, numbers, preferred_element_type=jnp.float32)  8.03 us
    mul x1, local copies, waits for them, and re-layouts, head_output(): grouped * grouped  5.15 us
  transfers between devices with their start and end apart: 4, of which 4 were waited for; matrix products, arithmetic and copies ran while one was open for 6% of the time, Pallas kernels for 0%

profile of v1, /device:TPU:0, one launch (start us, length us, event | category | flops | bytes accessed | tf_op | source)
XLA Modules:
  0.0 242.1 jit_solution(2006806133440303402)
XLA Ops:
  7.2 0.9 broadcast_bitcast_fusion.1
  8.1 0.7 broadcast_bitcast_fusion
  8.8 4.2 %fusion = f32[768,1024]{1,0:T(8,128)} fusion(bf16[768,1024]{1,0:T(8,128)(2,1)} %param.10, bf16[768,1024]{1,0:T(8,128)(2,1)} %param.9, f32[1024]{0:T(1024)S(1)} %bitcast.21), kind=kLoop, calls=%fused_computation.2 | loop fusion | flops 3932160 | bytes 6295552 | tf_op jit(solution)/shard_map/mul | solution.py:23
  13.0 5.2 %mul.92 = f32[768,4,256]{2,1,0:T(4,128)} reshape(f32[768,1024]{1,0:T(8,128)} %fusion) | data formatting | bytes 6291456 | tf_op jit(solution)/shard_map/mul | solution.py:23
  18.2 2.8 %reduce_sum.27 = f32[768,4]{1,0:T(8,128)S(1)} reduce(f32[768,4,256]{2,1,0:T(4,128)} %mul.92, f32[]{:T(128)} %constant.2.clone.1), dimensions={2}, to_apply=%region_0.0 | reduce | flops 783360 | bytes 3158020 | tf_op jit(solution)/shard_map/reduce_sum | solution.py:23
  21.1 1.0 mul.93
  22.1 0.8 copy.46
  22.8 0.6 copy-done.1
  23.5 0.5 copy-done.2
  24.0 0.9 fusion.2
  25.0 1.0 fusion.5
  26.0 2.4 fusion.1
  28.5 46.5 %reduce-scatter.3.cloned.1.call-done = f32[512,256]{0,1:T(8,128)} async-done(((f32[2048,256]{0,1:T(8,128)}), f32[512,256]{0,1:T(8,128)}) %reduce-scatter.3.cloned.1.call-update) | async-done | bytes 524304 | tf_op jit(solution)/shard_map/reduce_scatter | solution.py:50
  75.0 9.3 %reduce-scatter.5.cloned.1.call-done = f32[512,128]{0,1:T(8,128)} async-done(((f32[512,256]{0,1:T(8,128)}), f32[512,128]{0,1:T(8,128)}) %reduce-scatter.5.cloned.1.call-update) | async-done | bytes 262160 | tf_op jit(solution)/shard_map/reduce_scatter | solution.py:56
  84.4 0.8 copy.35
  85.2 1.8 copy.38
  87.0 2.9 %copy.39 = f32[1024,512]{0,1:T(8,128)} copy(f32[1024,512]{1,0:T(8,128)} %param.15) | data formatting | bytes 4194304 | tf_op args[6]
  89.9 23.9 %all-gather.6.cloned.1.call-done = f32[2048,128]{0,1:T(8,128)} async-done(((f32[512,128]{0,1:T(8,128)}), f32[2048,128]{0,1:T(8,128)}) %all-gather.6.cloned.1.call-update) | async-done | bytes 1048592 | tf_op jit(solution)/shard_map/all_gather | solution.py:12
  113.8 2.9 %reshape.25 = f32[4,512,128]{1,0,2:T(4,128)} reshape(f32[2048,128]{0,1:T(8,128)} %all-gather.6.cloned.1.call-done) | data formatting | bytes 2097152 | tf_op jit(solution)/shard_map/all_gather | solution.py:12
  116.7 2.5 %reduce_sum.28 = f32[512,128]{0,1:T(8,128)} reduce(f32[4,512,128]{1,0,2:T(4,128)} %reshape.25, f32[]{:T(128)} %constant.2.clone.1), dimensions={0}, to_apply=%region_3.0 | reduce | flops 196608 | bytes 1310724 | tf_op jit(solution)/shard_map/reduce_sum | solution.py:13
  119.3 2.6 %multiply_reduce_fusion = (f32[]{:T(128)}, f32[512,128]{0,1:T(8,128)S(1)}, f32[512,128]{0,1:T(8,128)}, f32[512,128]{0,1:T(8,128)}) fusion(f32[512,128]{0,1:T(8,128)} %reduce_sum.28, f32[512,128]{0,1:T(8,128)} %copy.38, f32[512,128]{0,1:T(8,128)} %copy.35), kind=kLoop, calls=%fused_computation.12 | loop fusion | flops 720895 | bytes 1572868 | tf_op jit(solution)/shard_map/reduce_sum | solution.py:61
  121.9 16.8 %psum.7 = f32[]{:T(128)} all-reduce(f32[]{:T(128)} %get-tuple-element.27), channel_id=1, replica_groups=mesh['fs'=4,'rep'=4,'tp'=2] {'fs','tp'}, use_global_device_ids=true, to_apply=%region_5.0 | all-reduce | flops 1 | bytes 8 | tf_op jit(solution)/shard_map/psum | solution.py:61
  139.4 2.2 all_gather.14
  141.6 0.8 copy-done.4
  142.4 2.9 %fusion.8 = f32[512,1024]{1,0:T(8,128)} fusion(bf16[1024,256]{1,0:T(8,128)(2,1)} %param.14, f32[512,256]{0,1:T(8,128)S(1)} %all_gather.14), kind=kOutput, calls=%fused_computation.19 | convolution fusion | flops 268566528 | bytes 3145728 | tf_op jit(solution)/shard_map/dot_general | solution.py:31
  145.3 5.7 %fusion.11 = (bf16[1024,512]{0,1:T(8,128)(2,1)}, f32[1024,512]{0,1:T(8,128)}, f32[1024,512]{0,1:T(8,128)}) fusion(f32[1024,512]{0,1:T(8,128)} %copy.39, f32[]{:T(128)S(6)} %div.19, f32[512,1024]{1,0:T(8,128)} %fusion.8, bf16[1024,256]{1,0:T(8,128)(2,1)} %param.14, f32[512,256]{0,1:T(8,128)} %copy-done.4), kind=kOutput, calls=%fused_computation.24 | convolution fusion | flops 271056896 | bytes 10485764 | tf_op jit(solution)/shard_map/dot_general | solution.py:33
  151.0 1.8 copy.44
  152.8 0.8 copy.43
  153.6 3.0 %copy.40 = f32[1024,512]{1,0:T(8,128)} copy(f32[1024,512]{0,1:T(8,128)} %get-tuple-element.26) | data formatting | bytes 4194304
  156.6 2.9 %copy.42 = f32[1024,512]{1,0:T(8,128)} copy(f32[1024,512]{0,1:T(8,128)} %get-tuple-element.31) | data formatting | bytes 4194304
  159.6 69.5 %all-gather.4.cloned.1.call-done = bf16[1024,2048]{0,1:T(8,128)(2,1)} async-done(((bf16[1024,512]{0,1:T(8,128)(2,1)}), bf16[1024,2048]{0,1:T(8,128)(2,1)}) %all-gather.4.cloned.1.call-update) | async-done | bytes 4194320 | tf_op jit(solution)/shard_map/all_gather | solution.py:69
  229.1 6.4 %copy.41 = bf16[1024,2048]{1,0:T(8,128)(2,1)} copy(bf16[1024,2048]{0,1:T(8,128)(2,1)} %all-gather.4.cloned.1.call-done) | data formatting | bytes 8388608
  (22 shorter events, 0.4 us)
Async XLA Ops:
  7.2 17.8 %copy-start = (bf16[768,2048]{1,0:T(8,128)(2,1)S(1)}, bf16[768,2048]{1,0:T(8,128)(2,1)}, u32[]{:S(2)}) copy-start(bf16[768,2048]{1,0:T(8,128)(2,1)} %param.13) | copy-start | bytes 9437188
  7.2 67.7 %reduce-scatter.3.cloned.1.call-start = ((), (), s32[]{:S(2)}) async-start(), calls=%async_computation.2 | async-start | bytes 2621440 | tf_op jit(solution)/shard_map/reduce_scatter | solution.py:50
  22.0 1.4 copy-start.1
  22.1 1.9 copy-start.2
  22.1 2.0 copy-start.3
  26.0 58.4 %copy-start.6 = (f32[512,128]{1,0:T(8,128)S(1)}, f32[512,128]{1,0:T(8,128)}, u32[]{:S(2)}) copy-start(f32[512,128]{1,0:T(8,128)} %param.16) | copy-start | bytes 786436
  28.4 55.9 %reduce-scatter.5.cloned.1.call-start = ((), (), s32[]{:S(2)}) async-start(), calls=%async_computation.3 | async-start | bytes 786432 | tf_op jit(solution)/shard_map/reduce_scatter | solution.py:56
  74.9 38.9 %all-gather.6.cloned.1.call-start = ((), (), s32[]{:S(2)}) async-start(), calls=%async_computation.5 | async-start | bytes 1310720 | tf_op jit(solution)/shard_map/all_gather | solution.py:12
  84.4 144.8 %all-gather.4.cloned.1.call-start = ((), (), s32[]{:S(2)}) async-start(), calls=%async_computation.4 | async-start | bytes 5242880 | tf_op jit(solution)/shard_map/all_gather | solution.py:69
  141.6 0.8 copy-start.4
  145.3 7.5 %copy-start.5 = (f32[512,128]{0,1:T(8,128)S(1)}, f32[512,128]{0,1:T(8,128)}, u32[]{:S(2)}) copy-start(f32[512,128]{0,1:T(8,128)} %get-tuple-element.30) | copy-start | bytes 786436
Sparse Core Ops, SparseCore 0:
  28.5 46.3 reduce-scatter.2
  77.2 7.1 reduce-scatter.4
  86.2 27.6 all-gather.5
  151.1 77.9 all-gather.3
